TPU v7x, 32 devices: a whole 2x2x4 slice. The times are simulated.
32 devices in a mesh: ra: 8 (over z, y), cb: 4 (over x, core).
Axes of the slice: x: 2, y: 2, z: 4, core: 2. Of those that a mesh axis runs over, the one named last changes fastest.
Arguments:
- tokens: bfloat16 [128, 2048], P(None, 'ra'), may hold values from -6 to 6
- pre_gain: float32 [2, 2048], P(None, 'ra'), may hold values from 0.1 to 1.9
- post_gain: float32 [2, 2048], P(None, 'ra'), may hold values from 0.1 to 1.9
- gate_weight: bfloat16 [2, 2048, 5632], P(None, 'ra', 'cb'), may hold values from -0.125 to 0.125
- up_weight: bfloat16 [2, 2048, 5632], P(None, 'ra', 'cb'), may hold values from -0.125 to 0.125
- down_weight: bfloat16 [2, 5632, 2048], P(None, 'cb', 'ra'), may hold values from -0.078125 to 0.078125
Outputs:
- mixed: bfloat16 [128, 2048], P(None, 'ra')
All inputs are finite; a program needn't handle non-finite values.
Results may differ from a plain program's by a relative error of at most 0.008.
Values may be sent and summed in bfloat16 or wider, within the bound.
A program may use at most 64 MiB of HBM per device.

v0:
```python
import jax
import jax.numpy as jnp
from jax import lax
from jax.sharding import PartitionSpec as P

D = 2048


epsilon = 1e-06
residual_scale = 0.25


def project(normed, gate_block, up_block, down_block):
    gate_part = jnp.dot(normed, gate_block, preferred_element_type=jnp.float32)
    up_part = jnp.dot(normed, up_block, preferred_element_type=jnp.float32)
    gate_sum, up_sum = lax.psum((gate_part, up_part), "ra")
    hidden = (jax.nn.silu(gate_sum) * up_sum).astype(jnp.bfloat16)
    partial_out = jnp.dot(hidden, down_block, preferred_element_type=jnp.float32)
    return lax.psum(partial_out, "cb")


def body(tokens, pre_gain, post_gain, gate_weight, up_weight, down_weight):
    stream = tokens.astype(jnp.float32)
    squares = jnp.zeros((stream.shape[0],), jnp.float32)
    squares = lax.psum(jnp.sum(stream * stream, axis=1), "ra")
    for sublayer in range(pre_gain.shape[0]):
        scale_in = lax.rsqrt(squares / D + epsilon)
        normed = (stream * scale_in[:, None] * pre_gain[sublayer]).astype(jnp.bfloat16)
        branch = project(normed, gate_weight[sublayer], up_weight[sublayer], down_weight[sublayer])
        gained = branch * post_gain[sublayer]
        branch_sq, gained_sq, cross_sum = lax.psum(
            (
                jnp.sum(branch * branch, axis=1),
                jnp.sum(gained * gained, axis=1),
                jnp.sum(stream * gained, axis=1),
            ),
            "ra",
        )
        scale_out = lax.rsqrt(branch_sq / D + epsilon)
        squares = (
            residual_scale * residual_scale * squares
            + 2.0 * residual_scale * scale_out * cross_sum
            + scale_out * scale_out * gained_sq
        )
        stream = residual_scale * stream + gained * scale_out[:, None]
    return stream.astype(jnp.bfloat16)


def solution(mesh):
    in_specs = (
        P(None, "ra"),
        P(None, "ra"),
        P(None, "ra"),
        P(None, "ra", "cb"),
        P(None, "ra", "cb"),
        P(None, "cb", "ra"),
    )
    out_specs = P(None, "ra")
    return jax.shard_map(body, mesh=mesh, in_specs=in_specs, out_specs=out_specs, check_vma=False)
```

profile of v0, /device:TPU:0, one launch (start us, length us, event | category | flops | bytes accessed | tf_op | source)
XLA Modules:
  0.0 326.6 jit_solution(7760830117557888802)
XLA Ops:
  6.5 0.0 copy-start
  6.5 0.0 copy-start.3
  6.5 0.0 all-reduce.14.cloned.1.call-start
  6.5 1.1 fusion.19
  7.6 23.2 %psum.77 = f32[128]{0:T(128)S(1)} all-reduce(f32[128]{0:T(128)S(1)} %fusion.19), channel_id=1, replica_groups=mesh['ra'=8,'cb'=4] {'ra'}, use_global_device_ids=true, to_apply=%region_1.0 | all-reduce | flops 128 | bytes 1024 | tf_op jit(solution)/shard_map/psum | solution.py:25
  30.8 0.8 fusion.28
  31.6 2.3 fusion.8
  33.9 0.0 copy-done
  33.9 0.0 copy-done.3
  33.9 1.2 fusion.10
  35.1 0.0 all-reduce.14.cloned.1.call-update
  35.1 0.0 all-reduce.8.cloned.1.call-start
  35.2 84.3 %all-reduce.14.cloned.1.call-done = (f32[128,1408]{1,0:T(8,128)}, f32[128,1408]{1,0:T(8,128)}) async-done(((f32[128,1408]{1,0:T(8,128)}, f32[128,1408]{1,0:T(8,128)}), (f32[128,1408]{1,0:T(8,128)}, f32[128,1408]{1,0:T(8,128)})) %all-reduce.14.cloned.1.call-update) | async-done | bytes 1441808 | tf_op jit(solution)/shard_map/psum | solution.py:16
  119.5 0.0 copy-start.4
  119.5 0.0 copy-start.2
  119.5 2.6 fusion.6
  122.2 0.0 all-reduce.8.cloned.1.call-update
  122.2 0.0 all-reduce.12.cloned.1.call-start
  122.3 0.0 copy-done.4
  122.3 31.0 %all-reduce.8.cloned.1.call-done = f32[128,256]{1,0:T(8,128)} async-done(((f32[128,256]{1,0:T(8,128)}), f32[128,256]{1,0:T(8,128)}) %all-reduce.8.cloned.1.call-update) | async-done | bytes 131088 | tf_op jit(solution)/shard_map/psum | solution.py:19
  153.3 0.0 copy-start.1
  153.3 1.1 fusion.22
  154.4 21.4 %all-reduce = (f32[128]{0:T(128)S(1)}, f32[128]{0:T(128)S(1)}, f32[128]{0:T(128)S(1)}) all-reduce(f32[128]{0:T(128)S(1)} %get-tuple-element.6, f32[128]{0:T(128)S(1)} %get-tuple-element.5, f32[128]{0:T(128)S(1)} %get-tuple-element.7), channel_id=1, replica_groups=mesh['ra'=8,'cb'=4] {'ra'}, use_global_device_ids=true, to_apply=%region_10.11 | all-reduce | flops 384 | bytes 3072 | tf_op jit(solution)/shard_map/psum | solution.py:31
  175.8 0.0 copy-done.2
  175.8 2.1 fusion.2
  177.9 0.0 copy-done.1
  177.9 0.0 copy-start.5
  177.9 1.2 fusion.4
  179.1 0.0 all-reduce.12.cloned.1.call-update
  179.2 0.0 all-reduce.10.cloned.1.call-start
  179.2 83.4 %all-reduce.12.cloned.1.call-done = (f32[128,1408]{1,0:T(8,128)}, f32[128,1408]{1,0:T(8,128)}) async-done(((f32[128,1408]{1,0:T(8,128)}, f32[128,1408]{1,0:T(8,128)}), (f32[128,1408]{1,0:T(8,128)}, f32[128,1408]{1,0:T(8,128)})) %all-reduce.12.cloned.1.call-update) | async-done | bytes 1441808 | tf_op jit(solution)/shard_map/psum | solution.py:16
  262.6 0.0 copy-done.5
  262.6 2.3 fusion
  264.9 0.0 all-reduce.10.cloned.1.call-update
  265.0 31.1 %all-reduce.10.cloned.1.call-done = f32[128,256]{1,0:T(8,128)} async-done(((f32[128,256]{1,0:T(8,128)}), f32[128,256]{1,0:T(8,128)}) %all-reduce.10.cloned.1.call-update) | async-done | bytes 131088 | tf_op jit(solution)/shard_map/psum | solution.py:19
  296.1 1.0 multiply_reduce_fusion
  297.1 21.4 %psum.87 = f32[128]{0:T(128)S(1)} all-reduce(f32[128]{0:T(128)S(1)} %multiply_reduce_fusion), channel_id=1, replica_groups=mesh['ra'=8,'cb'=4] {'ra'}, use_global_device_ids=true, to_apply=%region_15.16 | all-reduce | flops 128 | bytes 1024 | tf_op jit(solution)/shard_map/psum | solution.py:31
  318.4 1.6 add_convert_fusion
  (4 shorter events, 0.0 us)
Async XLA Ops:
  6.5 27.4 %copy-start = (bf16[128,256]{1,0:T(8,128)(2,1)S(1)}, bf16[128,256]{1,0:T(8,128)(2,1)}, u32[]{:S(2)}) copy-start(bf16[128,256]{1,0:T(8,128)(2,1)} %param.6) | copy-start | bytes 196612
  6.5 27.4 %copy-start.3 = (bf16[2,256,1408]{2,1,0:T(8,128)(2,1)S(1)}, bf16[2,256,1408]{2,1,0:T(8,128)(2,1)}, u32[]{:S(2)}) copy-start(bf16[2,256,1408]{2,1,0:T(8,128)(2,1)} %param.9) | copy-start | bytes 4325380
  6.5 113.0 %all-reduce.14.cloned.1.call-start = ((), (), s32[]{:S(2)}) async-start(), calls=%async_computation.3 | async-start | bytes 2883584 | tf_op jit(solution)/shard_map/psum | solution.py:16
  35.1 118.2 %all-reduce.8.cloned.1.call-start = ((), (), s32[]{:S(2)}) async-start(), calls=%async_computation | async-start | bytes 262144 | tf_op jit(solution)/shard_map/psum | solution.py:19
  119.5 2.7 copy-start.4
  119.5 56.3 %copy-start.2 = (bf16[2,256,1408]{2,1,0:T(8,128)(2,1)S(1)}, bf16[2,256,1408]{2,1,0:T(8,128)(2,1)}, u32[]{:S(2)}) copy-start(bf16[2,256,1408]{2,1,0:T(8,128)(2,1)} %param.10) | copy-start | bytes 4325380
  122.2 140.4 %all-reduce.12.cloned.1.call-start = ((), (), s32[]{:S(2)}) async-start(), calls=%async_computation.2 | async-start | bytes 2883584 | tf_op jit(solution)/shard_map/psum | solution.py:16
  153.3 24.6 %copy-start.1 = (f32[128,256]{1,0:T(8,128)S(1)}, f32[128,256]{1,0:T(8,128)}, u32[]{:S(2)}) copy-start(f32[128,256]{1,0:T(8,128)} %all-reduce.8.cloned.1.call-done) | copy-start | bytes 393220
  177.9 84.7 %copy-start.5 = (bf16[2,1408,256]{2,1,0:T(8,128)(2,1)S(1)}, bf16[2,1408,256]{2,1,0:T(8,128)(2,1)}, u32[]{:S(2)}) copy-start(bf16[2,1408,256]{2,1,0:T(8,128)(2,1)} %param.11) | copy-start | bytes 4325380
  179.2 116.9 %all-reduce.10.cloned.1.call-start = ((), (), s32[]{:S(2)}) async-start(), calls=%async_computation.1 | async-start | bytes 262144 | tf_op jit(solution)/shard_map/psum | solution.py:19
Sparse Core Ops, SparseCore 0:
  35.3 84.2 all-reduce.13
  122.3 30.9 all-reduce.7
  179.3 83.2 all-reduce.11
  265.1 30.9 all-reduce.9
where the time goes:
time: 327 us
  waiting for transfers between devices  230 us (70%)
  blocking collectives  65.9 us (20%)
  between operations  13.2 us (4%)
  matrix products  11.8 us (4%)
  other arithmetic  4.86 us (1%)
    psum x2, waiting for transfers between devices, project(): gate_sum, up_sum = lax.psum((gate_part, up_part), 'ra')  168 us
    psum x2, waiting for transfers between devices, project(): return lax.psum(partial_out, 'cb')  62.2 us
    psum x2, blocking collectives, body(): lax.psum((jnp.sum(branch * branch, axis=1), jnp.sum(gained * gained, axis...  42.7 us
    psum x1, blocking collectives, body(): squares = lax.psum(jnp.sum(stream * stream, axis=1), 'ra')  23.2 us
  transfers between devices with their start and end apart: 4, of which 4 were waited for; matrix products, arithmetic and copies ran while one was open for 0% of the time, Pallas kernels for 0%

commit v1 on v0

v1 whole, which is shorter than its diff:
```python
import functools

import jax
import jax.numpy as jnp
from jax import lax
from jax.experimental import pallas as pl
from jax.experimental.pallas import tpu as pltpu
from jax.sharding import PartitionSpec as P

EPS = 1e-06
RES = 0.25
LANES = 128
CHUNKS = 4
F32 = jnp.float32
BF16 = jnp.bfloat16


def plain_body(width, tokens, pre_gain, post_gain, gate_weight, up_weight, down_weight):
    stream = tokens.astype(F32)
    squares = lax.psum(jnp.sum(stream * stream, axis=1), "ra")
    for l in range(pre_gain.shape[0]):
        scale_in = lax.rsqrt(squares / width + EPS)
        normed = (stream * scale_in[:, None] * pre_gain[l]).astype(BF16)
        gate = jnp.dot(normed, gate_weight[l], preferred_element_type=F32)
        up = jnp.dot(normed, up_weight[l], preferred_element_type=F32)
        gate, up = lax.psum((gate, up), "ra")
        hidden = (jax.nn.silu(gate) * up).astype(BF16)
        branch = lax.psum(jnp.dot(hidden, down_weight[l], preferred_element_type=F32), "cb")
        gained = branch * post_gain[l]
        b_sq, g_sq, cross = lax.psum(
            (
                jnp.sum(branch * branch, axis=1),
                jnp.sum(gained * gained, axis=1),
                jnp.sum(stream * gained, axis=1),
            ),
            "ra",
        )
        scale_out = lax.rsqrt(b_sq / width + EPS)
        squares = RES * RES * squares + 2.0 * RES * scale_out * cross + scale_out * scale_out * g_sq
        stream = RES * stream + gained * scale_out[:, None]
    return stream.astype(BF16)


def kernel(
    R, Y, C, groups, width,
    tok, pre, post, gw_h, uw_h, dw_h, out,
    gw, uw, dw, normed, sq, st_s, st_r, y_s, y_r, own, z_s, z_r, hall, b_p, b_r, fin,
    w_sem, st_ss, st_rs, y_ss, y_rs, z_ss, z_rs, hz_ss, hz_rs, hy_ss, hy_rs, b_ss, b_rs, n_ss, n_rs,
):
    Z = R // Y
    L = pre.shape[0]
    T = tok.shape[0]
    G = len(groups)
    tz = T // R
    ty = T // Y
    tc = T // C
    per = ty // tc
    ra = lax.axis_index("ra")
    c = lax.axis_index("cb")
    z = ra // Y
    y = lax.rem(ra, Y)

    loads = []
    for l in range(L):
        for k, (src, dst) in enumerate(((gw_h, gw), (uw_h, uw), (dw_h, dw))):
            cp = pltpu.make_async_copy(src.at[l], dst.at[l], w_sem.at[l, k])
            cp.start()
            loads.append(cp)

    bar = pltpu.get_barrier_semaphore()
    for s in range(1, R):
        pl.semaphore_signal(bar, inc=1, device_id={"ra": lax.rem(ra + s, R)}, device_id_type=pl.DeviceIdType.MESH)
    for s in range(1, C):
        pl.semaphore_signal(bar, inc=1, device_id={"cb": lax.rem(c + s, C)}, device_id_type=pl.DeviceIdType.MESH)

    sends = []

    def push(src, dst, ss, rs, axis, where):
        cp = pltpu.make_async_remote_copy(
            src_ref=src, dst_ref=dst, send_sem=ss, recv_sem=rs,
            device_id={axis: where}, device_id_type=pl.DeviceIdType.MESH,
        )
        cp.start()
        sends.append(cp)
        return cp

    def z_at(s):
        return lax.rem(z + s, Z) * Y + y

    def y_at(s):
        return z * Y + lax.rem(y + s, Y)

    def share_stats(i, columns):
        rows = columns[0].shape[0]
        lane = lax.broadcasted_iota(jnp.int32, (rows, LANES), 1)
        packed = jnp.zeros((rows, LANES), F32)
        for k, col in enumerate(columns):
            packed = jnp.where(lane == k, col, packed)
        if rows < LANES:
            packed = jnp.concatenate([packed, jnp.zeros((LANES - rows, LANES), F32)], axis=0)
        st_s[i] = packed.T[:8]
        cps = [
            push(st_s.at[i], st_r.at[i, s - 1], st_ss.at[i, s - 1], st_rs.at[i, s - 1], "ra", lax.rem(ra + s, R))
            for s in range(1, R)
        ]
        total = st_s[i]
        for s, cp in enumerate(cps):
            cp.wait_recv()
            total = total + st_r[i, s]
        turned = jnp.concatenate([total, jnp.zeros((LANES - 8, LANES), F32)], axis=0).T
        return [turned[:rows, k : k + 1] for k in range(len(columns))]

    tokens = tok[...].astype(F32)
    local_sq = jnp.sum(tokens * tokens, axis=1, keepdims=True)
    pl.semaphore_wait(bar, R + C - 2)

    (squares_all,) = share_stats(0, [local_sq])
    sq[...] = jnp.broadcast_to(squares_all, (T, LANES)).reshape(C, tc, LANES)
    first = (tokens * lax.rsqrt(squares_all / width + EPS) * pre[0:1, :]).astype(BF16)
    normed[0] = first.reshape(C, tc, first.shape[1])

    squares = sq[c][:, 0:1]
    stream = tok[pl.ds(pl.multiple_of(c * tc, tc), tc), :].astype(F32)

    for l in range(L):
        loads[3 * l].wait()
        loads[3 * l + 1].wait()

        def partial(half, b0, nb):
            rows = normed[l, pl.ds(half * per, per)].reshape(ty, normed.shape[-1])
            cols = slice(b0 * LANES, (b0 + nb) * LANES)
            return (
                jnp.dot(rows, gw[l, :, cols], preferred_element_type=F32),
                jnp.dot(rows, uw[l, :, cols], preferred_element_type=F32),
            )

        y_cp, z_cp, hz_cp, hy_cp = {}, {}, {}, {}

        def stage_a(g):
            b0, nb = groups[g]
            for s in range(1, Y):
                ga, ua = partial(lax.rem(y + s, Y), b0, nb)
                for i in range(nb):
                    y_s[l, s - 1, b0 + i, :, :LANES] = ga[:, i * LANES : (i + 1) * LANES].astype(BF16)
                    y_s[l, s - 1, b0 + i, :, LANES:] = ua[:, i * LANES : (i + 1) * LANES].astype(BF16)
                y_cp[g, s] = push(
                    y_s.at[l, s - 1, pl.ds(b0, nb)], y_r.at[l, s - 1, pl.ds(b0, nb)],
                    y_ss.at[l, g, s - 1], y_rs.at[l, g, s - 1], "ra", y_at(s),
                )

        def stage_a2(g):
            b0, nb = groups[g]
            ga, ua = partial(y, b0, nb)
            for i in range(nb):
                own[b0 + i, :, :LANES] = ga[:, i * LANES : (i + 1) * LANES]
                own[b0 + i, :, LANES:] = ua[:, i * LANES : (i + 1) * LANES]

        def stage_b(g):
            b0, nb = groups[g]
            total = own[b0 : b0 + nb]
            for s in range(1, Y):
                y_cp[g, s].wait_recv()
                total = total + y_r[l, s - 1, b0 : b0 + nb].astype(F32)
            own[b0 : b0 + nb] = total
            low = total.astype(BF16)
            for q in range(Z):
                z_s[l, q, b0 : b0 + nb] = low[:, q * tz : (q + 1) * tz, :]
            for s in range(1, Z):
                z_cp[g, s] = push(
                    z_s.at[l, lax.rem(z + s, Z), pl.ds(b0, nb)], z_r.at[l, s - 1, pl.ds(b0, nb)],
                    z_ss.at[l, g, s - 1], z_rs.at[l, g, s - 1], "ra", z_at(s),
                )

        def stage_c(g):
            b0, nb = groups[g]
            total = own[b0 : b0 + nb, pl.ds(pl.multiple_of(z * tz, tz), tz), :]
            for s in range(1, Z):
                z_cp[g, s].wait_recv()
                total = total + z_r[l, s - 1, b0 : b0 + nb].astype(F32)
            gate, up = total[:, :, :LANES], total[:, :, LANES:]
            hall[l, y, z, b0 : b0 + nb] = (gate / (1.0 + jnp.exp(-gate)) * up).astype(BF16)
            mine = hall.at[l, y, z, pl.ds(b0, nb)]
            for s in range(1, Z):
                hz_cp[g, s] = push(mine, mine, hz_ss.at[l, g, s - 1], hz_rs.at[l, g, s - 1], "ra", z_at(s))
            for s in range(1, Y):
                hy_cp[g, 0, s] = push(mine, mine, hy_ss.at[l, g, 0, s - 1], hy_rs.at[l, g, 0, s - 1], "ra", y_at(s))

        def stage_d(g):
            b0, nb = groups[g]
            for r in range(1, Z):
                hz_cp[g, r].wait_recv()
                got = hall.at[l, y, lax.rem(z + Z - r, Z), pl.ds(b0, nb)]
                for s in range(1, Y):
                    hy_cp[g, r, s] = push(got, got, hy_ss.at[l, g, r, s - 1], hy_rs.at[l, g, r, s - 1], "ra", y_at(s))

        def stage_e(g, acc):
            b0, nb = groups[g]
            for r in range(Z):
                for s in range(1, Y):
                    hy_cp[g, r, s].wait_recv()
            lhs = jnp.concatenate([hall[l, :, :, b0 + i].reshape(T, LANES) for i in range(nb)], axis=1)
            part = jnp.dot(lhs, dw[l, b0 * LANES : (b0 + nb) * LANES, :], preferred_element_type=F32)
            return part if acc is None else acc + part

        for g in range(G):
            stage_a(g)
        for g in range(G):
            stage_a2(g)
        acc = None
        for t in range(G + 3):
            if t < G:
                stage_b(t)
            if 0 <= t - 1 < G:
                stage_c(t - 1)
            if 0 <= t - 2 < G:
                stage_d(t - 2)
            if 0 <= t - 3 < G:
                if t == 3:
                    loads[3 * l + 2].wait()
                acc = stage_e(t - 3, acc)

        b_p[l] = acc.reshape(C, tc, acc.shape[1])
        cps = []
        for s in range(1, C):
            to = lax.rem(c + s, C)
            cps.append(push(b_p.at[l, to], b_r.at[l, s - 1], b_ss.at[l, s - 1], b_rs.at[l, s - 1], "cb", to))
        branch = b_p[l, c]
        for s, cp in enumerate(cps):
            cp.wait_recv()
            branch = branch + b_r[l, s]

        gained = branch * post[l : l + 1, :]
        b_sq, g_sq, cross = share_stats(
            l + 1,
            [
                jnp.sum(branch * branch, axis=1, keepdims=True),
                jnp.sum(gained * gained, axis=1, keepdims=True),
                jnp.sum(stream * gained, axis=1, keepdims=True),
            ],
        )
        scale_out = lax.rsqrt(b_sq / width + EPS)
        squares = RES * RES * squares + 2.0 * RES * scale_out * cross + scale_out * scale_out * g_sq
        stream = RES * stream + gained * scale_out
        if l + 1 < L:
            scale_in = lax.rsqrt(squares / width + EPS)
            normed[l + 1, c] = (stream * scale_in * pre[l + 1 : l + 2, :]).astype(BF16)
            mine = normed.at[l + 1, c]
        else:
            fin[c] = stream.astype(BF16)
            mine = fin.at[c]
        cps = [
            push(mine, mine, n_ss.at[l, s - 1], n_rs.at[l, s - 1], "cb", lax.rem(c + s, C))
            for s in range(1, C)
        ]
        for cp in cps:
            cp.wait_recv()

    out[...] = fin[...].reshape(T, fin.shape[-1])
    for cp in sends:
        cp.wait_send()


def fused_body(R, Y, C, width, tokens, pre_gain, post_gain, gate_weight, up_weight, down_weight):
    L = pre_gain.shape[0]
    T, d = tokens.shape
    f = gate_weight.shape[2]
    NB = f // LANES
    Z = R // Y
    tz, ty, tc = T // R, T // Y, T // C
    G = min(CHUNKS, NB)
    groups, at = [], 0
    for g in range(G):
        nb = NB // G + (1 if g < NB % G else 0)
        groups.append((at, nb))
        at += nb
    dma = pltpu.SemaphoreType.DMA
    vm = pl.BlockSpec(memory_space=pltpu.VMEM)
    hbm = pl.BlockSpec(memory_space=pl.ANY)
    scratch = [
        pltpu.VMEM((L, d, f), BF16),
        pltpu.VMEM((L, d, f), BF16),
        pltpu.VMEM((L, f, d), BF16),
        pltpu.VMEM((L, C, tc, d), BF16),
        pltpu.VMEM((C, tc, LANES), F32),
        pltpu.VMEM((L + 1, 8, LANES), F32),
        pltpu.VMEM((L + 1, R - 1, 8, LANES), F32),
        pltpu.VMEM((L, Y - 1, NB, ty, 2 * LANES), BF16),
        pltpu.VMEM((L, Y - 1, NB, ty, 2 * LANES), BF16),
        pltpu.VMEM((NB, ty, 2 * LANES), F32),
        pltpu.VMEM((L, Z, NB, tz, 2 * LANES), BF16),
        pltpu.VMEM((L, Z - 1, NB, tz, 2 * LANES), BF16),
        pltpu.VMEM((L, Y, Z, NB, tz, LANES), BF16),
        pltpu.VMEM((L, C, tc, d), F32),
        pltpu.VMEM((L, C - 1, tc, d), F32),
        pltpu.VMEM((C, tc, d), BF16),
        dma((L, 3)),
        dma((L + 1, R - 1)), dma((L + 1, R - 1)),
        dma((L, G, Y - 1)), dma((L, G, Y - 1)),
        dma((L, G, Z - 1)), dma((L, G, Z - 1)),
        dma((L, G, Z - 1)), dma((L, G, Z - 1)),
        dma((L, G, Z, Y - 1)), dma((L, G, Z, Y - 1)),
        dma((L, C - 1)), dma((L, C - 1)),
        dma((L, C - 1)), dma((L, C - 1)),
    ]
    return pl.pallas_call(
        functools.partial(kernel, R, Y, C, tuple(groups), width),
        out_shape=jax.ShapeDtypeStruct((T, d), BF16),
        in_specs=[vm, vm, vm, hbm, hbm, hbm],
        out_specs=vm,
        scratch_shapes=scratch,
        compiler_params=pltpu.CompilerParams(
            collective_id=0, has_side_effects=True, vmem_limit_bytes=48 * 1024 * 1024
        ),
        name="window",
    )(tokens, pre_gain, post_gain, gate_weight, up_weight, down_weight)


def solution(mesh):
    R, C = mesh.shape["ra"], mesh.shape["cb"]
    Y = max(C // 2, 1)
    if R % Y:
        Y = 1

    def body(*arrays):
        tokens, gate_weight = arrays[0], arrays[3]
        T, d = tokens.shape
        width = d * R
        f = gate_weight.shape[2]
        fits = (
            1 < Y < R and C > 1 and T <= LANES and T % (16 * R) == 0 and T % (16 * C) == 0
            and (T // Y) % (T // C) == 0 and d % LANES == 0 and f % LANES == 0
        )
        if fits:
            return fused_body(R, Y, C, width, *arrays)
        return plain_body(width, *arrays)

    in_specs = (
        P(None, "ra"),
        P(None, "ra"),
        P(None, "ra"),
        P(None, "ra", "cb"),
        P(None, "ra", "cb"),
        P(None, "cb", "ra"),
    )
    return jax.shard_map(body, mesh=mesh, in_specs=in_specs, out_specs=P(None, "ra"), check_vma=False)
```

time: 327 us -> 88.7 us (0.27)
  waiting for transfers between devices: 230 us -> 0 us
  Pallas kernels: 0 us -> 81.5 us
  blocking collectives: 65.9 us -> 0 us
  between operations: 13.2 us -> 0.02 us
  matrix products: 11.8 us -> 0 us
  local copies, waits for them, and re-layouts: 0.79 us -> 6.92 us
  other arithmetic: 4.86 us -> 0 us
    psum x4 -> x0, waiting for transfers between devices: 230 us -> none  [the longest x2 168 us: project(): gate_sum, up_sum = lax.psum((gate_part, up_part), 'ra')]
    pallas_call x0 -> x1, Pallas kernels: none -> 81.5 us  [fused_body(): pl.pallas_call(functools.partial(kernel, R, Y, C, tuple(groups), width),...]
    psum x3 -> x0, blocking collectives: 65.9 us -> none  [the longest x2 42.7 us: body(): lax.psum((jnp.sum(branch * branch, axis=1), jnp.sum(gained * gained, axis...]
    dot_general x6 -> x0, matrix products: 11.8 us -> none  [the longest x2 4.98 us: project(): jnp.dot(hidden, down_block, preferred_element_type=jnp.float32)]
    unnamed x12 -> x13, local copies, waits for them, and re-layouts: 0.02 us -> 6.92 us
  transfers between devices with their start and end apart: 4 -> 0, of which waited for: 4 -> 0; matrix products, arithmetic and copies ran while one was open for 0% -> 0% of each run, Pallas kernels for 0% -> 0%
where the time goes in v1:
time: 88.7 us; the launch traced here: 88.4 us
  Pallas kernels  81.5 us (92%)
  local copies, waits for them, and re-layouts  6.92 us (8%)
    pallas_call x1, Pallas kernels, fused_body(): pl.pallas_call(functools.partial(kernel, R, Y, C, tuple(groups), width),...  81.5 us
    unnamed x13, local copies, waits for them, and re-layouts  6.92 us

profile of v1, /device:TPU:0, one launch (start us, length us, event | category | flops | bytes accessed | tf_op | source)
XLA Modules:
  0.0 88.4 jit_solution(8536938236101672128)
XLA Ops:
  0.0 0.0 copy-start
  0.0 1.4 %copy-done = bf16[2,256,1408]{2,1,0:T(8,128)(2,1)S(1)} copy-done((bf16[2,256,1408]{2,1,0:T(8,128)(2,1)S(1)}, bf16[2,256,1408]{2,1,0:T(8,128)(2,1)}, u32[]{:S(2)}) %copy-start) | copy-done | bytes 1441816
  1.4 0.0 copy-start.1
  1.4 1.4 %copy-done.1 = bf16[2,256,1408]{2,1,0:T(8,128)(2,1)S(1)} copy-done((bf16[2,256,1408]{2,1,0:T(8,128)(2,1)S(1)}, bf16[2,256,1408]{2,1,0:T(8,128)(2,1)}, u32[]{:S(2)}) %copy-start.1) | copy-done | bytes 1441816
  2.7 0.0 copy-start.2
  2.7 1.4 %copy-done.2 = bf16[2,1408,256]{2,1,0:T(8,128)(2,1)S(1)} copy-done((bf16[2,1408,256]{2,1,0:T(8,128)(2,1)S(1)}, bf16[2,1408,256]{2,1,0:T(8,128)(2,1)}, u32[]{:S(2)}) %copy-start.2) | copy-done | bytes 1441816
  4.1 0.0 copy-start.3
  4.1 0.8 copy-done.3
  4.9 0.0 copy-start.4
  4.9 0.7 copy-done.4
  5.6 0.0 copy-start.5
  5.6 0.7 copy-done.5
  6.3 81.5 %window.1 = bf16[128,256]{1,0:T(8,128)(2,1)S(1)} custom-call(bf16[128,256]{1,0:T(8,128)(2,1)S(1)} %copy-done.3, f32[2,256]{1,0:T(2,128)S(1)} %copy-done.4, f32[2,256]{1,0:T(2,128)S(1)} %copy-done.5, bf16[2,256,1408]{2,1,0:T(8,128)(2,1)S(1)} %copy-done, bf16[2,256,1408]{2,1,0:T(8,128)(2,1)S(1)} %copy-done.1, bf16[2,1408,256]{2,1,0:T(8,128)(2,1)S(1)} %copy-done.2), custom_call_target="tpu_custom_call" | custom-call | tf_op jit(solution)/shard_map/window/pallas_call | solution.py:305
  87.8 0.6 copy.8
Async XLA Ops:
  0.0 1.4 %copy-start = (bf16[2,256,1408]{2,1,0:T(8,128)(2,1)S(1)}, bf16[2,256,1408]{2,1,0:T(8,128)(2,1)}, u32[]{:S(2)}) copy-start(bf16[2,256,1408]{2,1,0:T(8,128)(2,1)} %gw_h.1) | copy-start | bytes 4325380
  1.4 1.4 %copy-start.1 = (bf16[2,256,1408]{2,1,0:T(8,128)(2,1)S(1)}, bf16[2,256,1408]{2,1,0:T(8,128)(2,1)}, u32[]{:S(2)}) copy-start(bf16[2,256,1408]{2,1,0:T(8,128)(2,1)} %uw_h.1) | copy-start | bytes 4325380
  2.7 1.4 %copy-start.2 = (bf16[2,1408,256]{2,1,0:T(8,128)(2,1)S(1)}, bf16[2,1408,256]{2,1,0:T(8,128)(2,1)}, u32[]{:S(2)}) copy-start(bf16[2,1408,256]{2,1,0:T(8,128)(2,1)} %dw_h.1) | copy-start | bytes 4325380
  4.1 0.8 copy-start.3
  4.9 0.7 copy-start.4
  5.6 0.7 copy-start.5

commit v2 on v1

--- a/solution.py
+++ b/solution.py
@@ -10,7 +10,7 @@
 EPS = 1e-06
 RES = 0.25
 LANES = 128
-CHUNKS = 4
+CHUNKS = 3
 F32 = jnp.float32
 BF16 = jnp.bfloat16
 
@@ -43,9 +43,9 @@
 
 def kernel(
     R, Y, C, groups, width,
-    tok, pre, post, gw_h, uw_h, dw_h, out,
-    gw, uw, dw, normed, sq, st_s, st_r, y_s, y_r, own, z_s, z_r, hall, b_p, b_r, fin,
-    w_sem, st_ss, st_rs, y_ss, y_rs, z_ss, z_rs, hz_ss, hz_rs, hy_ss, hy_rs, b_ss, b_rs, n_ss, n_rs,
+    tok_h, pre_h, post_h, gw_h, uw_h, dw_h, out,
+    tok, pre, post, gw, uw, dw, normed, sq, st_s, st_r, y_s, y_r, own, z_s, z_r, hall, b_p, b_r, fin,
+    i_sem, w_sem, st_ss, st_rs, y_ss, y_rs, z_ss, z_rs, hz_ss, hz_rs, hy_ss, hy_rs, b_ss, b_rs, n_ss, n_rs,
 ):
     Z = R // Y
     L = pre.shape[0]
@@ -60,6 +60,11 @@
     z = ra // Y
     y = lax.rem(ra, Y)
 
+    small = []
+    for k, (src, dst) in enumerate(((tok_h, tok), (pre_h, pre), (post_h, post))):
+        cp = pltpu.make_async_copy(src, dst, i_sem.at[k])
+        cp.start()
+        small.append(cp)
     loads = []
     for l in range(L):
         for k, (src, dst) in enumerate(((gw_h, gw), (uw_h, uw), (dw_h, dw))):
@@ -110,6 +115,8 @@
         turned = jnp.concatenate([total, jnp.zeros((LANES - 8, LANES), F32)], axis=0).T
         return [turned[:rows, k : k + 1] for k in range(len(columns))]
 
+    for cp in small:
+        cp.wait()
     tokens = tok[...].astype(F32)
     local_sq = jnp.sum(tokens * tokens, axis=1, keepdims=True)
     pl.semaphore_wait(bar, R + C - 2)
@@ -275,8 +282,11 @@
         at += nb
     dma = pltpu.SemaphoreType.DMA
     vm = pl.BlockSpec(memory_space=pltpu.VMEM)
-    hbm = pl.BlockSpec(memory_space=pl.ANY)
+    hbm = pl.BlockSpec(memory_space=pltpu.HBM)
     scratch = [
+        pltpu.VMEM((T, d), BF16),
+        pltpu.VMEM((L, d), F32),
+        pltpu.VMEM((L, d), F32),
         pltpu.VMEM((L, d, f), BF16),
         pltpu.VMEM((L, d, f), BF16),
         pltpu.VMEM((L, f, d), BF16),
@@ -293,6 +303,7 @@
         pltpu.VMEM((L, C, tc, d), F32),
         pltpu.VMEM((L, C - 1, tc, d), F32),
         pltpu.VMEM((C, tc, d), BF16),
+        dma((3,)),
         dma((L, 3)),
         dma((L + 1, R - 1)), dma((L + 1, R - 1)),
         dma((L, G, Y - 1)), dma((L, G, Y - 1)),
@@ -305,11 +316,11 @@
     return pl.pallas_call(
         functools.partial(kernel, R, Y, C, tuple(groups), width),
         out_shape=jax.ShapeDtypeStruct((T, d), BF16),
-        in_specs=[vm, vm, vm, hbm, hbm, hbm],
+        in_specs=[hbm] * 6,
         out_specs=vm,
         scratch_shapes=scratch,
         compiler_params=pltpu.CompilerParams(
-            collective_id=0, has_side_effects=True, vmem_limit_bytes=48 * 1024 * 1024
+            collective_id=0, has_side_effects=True, vmem_limit_bytes=67043328
         ),
         name="window",
     )(tokens, pre_gain, post_gain, gate_weight, up_weight, down_weight)

time: 88.7 us -> 81.8 us (0.922)
  local copies, waits for them, and re-layouts: 6.92 us -> 1.47 us
  Pallas kernels: 81.5 us -> 80.2 us
    unnamed x13 -> x1, local copies, waits for them, and re-layouts: 6.92 us -> 1.47 us
    pallas_call x1, Pallas kernels: 81.5 us -> 80.2 us  [fused_body(): pl.pallas_call(functools.partial(kernel, R, Y, C, tuple(groups), width),...]
where the time goes in v2:
time: 81.8 us; the launch traced here: 81.7 us
  Pallas kernels  80.2 us (98%)
  local copies, waits for them, and re-layouts  1.47 us (2%)
    pallas_call x1, Pallas kernels, fused_body(): pl.pallas_call(functools.partial(kernel, R, Y, C, tuple(groups), width),...  80.2 us

profile of v2, /device:TPU:0, one launch (start us, length us, event | category | flops | bytes accessed | tf_op | source)
XLA Modules:
  0.0 81.7 jit_solution(3178558352952196027)
XLA Ops:
  0.0 80.2 %window.1 = bf16[128,256]{1,0:T(8,128)(2,1)} custom-call(bf16[128,256]{1,0:T(8,128)(2,1)} %tok_h.1, f32[2,256]{1,0:T(2,128)} %pre_h.1, f32[2,256]{1,0:T(2,128)} %post_h.1, bf16[2,256,1408]{2,1,0:T(8,128)(2,1)} %gw_h.1, bf16[2,256,1408]{2,1,0:T(8,128)(2,1)} %uw_h.1, bf16[2,1408,256]{2,1,0:T(8,128)(2,1)} %dw_h.1), custom_call_target="tpu_custom_call" | custom-call | tf_op jit(solution)/shard_map/window/pallas_call | solution.py:316
  80.2 1.5 %copy.8 = bf16[128,256]{1,0:T(8,128)(2,1)} copy(bf16[128,256]{1,0:T(8,128)(2,1)} %window.1) | data formatting | bytes 131072

commit v3 on v2

--- a/solution.py
+++ b/solution.py
@@ -10,7 +10,6 @@
 EPS = 1e-06
 RES = 0.25
 LANES = 128
-CHUNKS = 3
 F32 = jnp.float32
 BF16 = jnp.bfloat16
 
@@ -274,10 +273,12 @@
     NB = f // LANES
     Z = R // Y
     tz, ty, tc = T // R, T // Y, T // C
-    G = min(CHUNKS, NB)
+    head = max(NB // 5, 1) if NB > 2 else 0
+    rest = NB - head
+    sizes = [n for n in (head, rest - rest // 2, rest // 2) if n]
+    G = len(sizes)
     groups, at = [], 0
-    for g in range(G):
-        nb = NB // G + (1 if g < NB % G else 0)
+    for nb in sizes:
         groups.append((at, nb))
         at += nb
     dma = pltpu.SemaphoreType.DMA

time: 81.8 us -> 80.1 us (0.979)
  Pallas kernels: 80.2 us -> 78.5 us
    pallas_call x1, Pallas kernels: 80.2 us -> 78.5 us  [fused_body(): pl.pallas_call(functools.partial(kernel, R, Y, C, tuple(groups), width),...]
where the time goes in v3:
time: 80.1 us; the launch traced here: 80 us
  Pallas kernels  78.5 us (98%)
  local copies, waits for them, and re-layouts  1.47 us (2%)
    pallas_call x1, Pallas kernels, fused_body(): pl.pallas_call(functools.partial(kernel, R, Y, C, tuple(groups), width),...  78.5 us

profile of v3, /device:TPU:0, one launch (start us, length us, event | category | flops | bytes accessed | tf_op | source)
XLA Modules:
  0.0 80.0 jit_solution(8663049925744162966)
XLA Ops:
  0.0 78.5 %window.1 = bf16[128,256]{1,0:T(8,128)(2,1)} custom-call(bf16[128,256]{1,0:T(8,128)(2,1)} %tok_h.1, f32[2,256]{1,0:T(2,128)} %pre_h.1, f32[2,256]{1,0:T(2,128)} %post_h.1, bf16[2,256,1408]{2,1,0:T(8,128)(2,1)} %gw_h.1, bf16[2,256,1408]{2,1,0:T(8,128)(2,1)} %uw_h.1, bf16[2,1408,256]{2,1,0:T(8,128)(2,1)} %dw_h.1), custom_call_target="tpu_custom_call" | custom-call | tf_op jit(solution)/shard_map/window/pallas_call | solution.py:317
  78.5 1.5 %copy.8 = bf16[128,256]{1,0:T(8,128)(2,1)} copy(bf16[128,256]{1,0:T(8,128)(2,1)} %window.1) | data formatting | bytes 131072

commit v4 on v3

--- a/solution.py
+++ b/solution.py
@@ -210,12 +210,13 @@
 
         for g in range(G):
             stage_a(g)
-        for g in range(G):
-            stage_a2(g)
+        stage_a2(0)
         acc = None
         for t in range(G + 3):
             if t < G:
                 stage_b(t)
+                if t + 1 < G:
+                    stage_a2(t + 1)
             if 0 <= t - 1 < G:
                 stage_c(t - 1)
             if 0 <= t - 2 < G:

time: 80.1 us -> 79.9 us (level)
  no operation moved by 1% of the time
where the time goes in v4:
time: 79.9 us; the launch traced here: 79.7 us
  Pallas kernels  78.2 us (98%)
  local copies, waits for them, and re-layouts  1.47 us (2%)
    pallas_call x1, Pallas kernels, fused_body(): pl.pallas_call(functools.partial(kernel, R, Y, C, tuple(groups), width),...  78.2 us

profile of v4, /device:TPU:0, one launch (start us, length us, event | category | flops | bytes accessed | tf_op | source)
XLA Modules:
  0.0 79.7 jit_solution(12470806833070339725)
XLA Ops:
  0.0 78.2 %window.1 = bf16[128,256]{1,0:T(8,128)(2,1)} custom-call(bf16[128,256]{1,0:T(8,128)(2,1)} %tok_h.1, f32[2,256]{1,0:T(2,128)} %pre_h.1, f32[2,256]{1,0:T(2,128)} %post_h.1, bf16[2,256,1408]{2,1,0:T(8,128)(2,1)} %gw_h.1, bf16[2,256,1408]{2,1,0:T(8,128)(2,1)} %uw_h.1, bf16[2,1408,256]{2,1,0:T(8,128)(2,1)} %dw_h.1), custom_call_target="tpu_custom_call" | custom-call | tf_op jit(solution)/shard_map/window/pallas_call | solution.py:318
  78.2 1.5 %copy.8 = bf16[128,256]{1,0:T(8,128)(2,1)} copy(bf16[128,256]{1,0:T(8,128)(2,1)} %window.1) | data formatting | bytes 131072
